TPU v7x, 32 devices: a whole 2x2x4 slice. The times are simulated.
32 devices in a mesh: grp: 2 (over y), sp: 4 (over z), tp: 4 (over x, core).
Axes of the slice: x: 2, y: 2, z: 4, core: 2. Of those that a mesh axis runs over, the one named last changes fastest.
Arguments:
- residual: bfloat16 [2048, 2048], P(('grp', 'sp')), parts along dimension 0, may hold values from -34 to 34
- queries: bfloat16 [2048, 1024], P(('grp', 'sp'), 'tp'), parts along dimension 0, may hold values from -400 to 400
- keys: bfloat16 [2048, 512], P(('grp', 'sp'), 'tp'), parts along dimension 0, may hold values from -8 to 8
- values: bfloat16 [2048, 512], P(('grp', 'sp'), 'tp'), parts along dimension 0, may hold values from -6 to 6
- segments: int32 [2048], P(('grp', 'sp')), parts along dimension 0, may hold values from 0 to 2, never falling along the last dimension, each value on 1 to 768 neighbouring positions
- routes: int32 [2048, 2], P(('grp', 'sp')), parts along dimension 0, may hold values from 0 to 3, all different within a row; in each aligned block of 256 rows (0 to 255, 256 to 511, ...) at most 256 rows name the same one
- route_weight: float32 [2048, 2], P(('grp', 'sp')), parts along dimension 0, may hold values from 0.3 to 3
- sinks: float32 [16], P('tp'), may hold values from 1 to 6
- out_weight: bfloat16 [1024, 2048], P('tp'), may hold values from -1 to 1
- norm_gain: float32 [2048], replicated, may hold values from 0.1 to 1.9
- expert_gate: bfloat16 [4, 2048, 1024], P('sp', None, 'tp'), may hold values from -0.125 to 0.125
- expert_up: bfloat16 [4, 2048, 1024], P('sp', None, 'tp'), may hold values from -0.125 to 0.125
- expert_down: bfloat16 [4, 1024, 2048], P('sp', None, 'tp'), may hold values from -0.1875 to 0.1875
- shared_gate: bfloat16 [2048, 1024], P(None, 'tp'), may hold values from -0.125 to 0.125
- shared_up: bfloat16 [2048, 1024], P(None, 'tp'), may hold values from -0.125 to 0.125
- shared_down: bfloat16 [1024, 2048], P(None, 'tp'), may hold values from -0.1875 to 0.1875
Outputs:
- mixed: bfloat16 [2048, 2048], P(('grp', 'sp'), 'tp'), parts along dimension 0
There are 2 independent parts, one for each index of `grp`. A program takes and returns all parts, laid end to end along the dimension named above; an argument that names none is the same for every part. Nothing has to cross between parts.
Inputs may be any that keep to these rules, and one draw needn't show every extreme that they name: `routes`: each row names 2 different experts. In the rows of one device no expert is named by more than 256 rows, and in some device's rows an expert is named by exactly 256. `segments`: document numbers never fall along the positions; every document spans 1 to 768 positions and one spans exactly 768.
All inputs are finite; a program needn't handle non-finite values.
Results may differ from a plain program's by a relative error of at most 0.0065.
Values may be sent and summed in bfloat16 or wider, within the bound.
A program may use at most 64 MiB of HBM per device.

v0:
```python
import jax
import jax.numpy as jnp
from jax import lax
from jax.sharding import PartitionSpec as P

HEAD_DIM = 64
WINDOW = 128
epsilon = 1e-06


def passed_along(value, axis, steps):
    count = lax.axis_size(axis)
    leading, last = (max(0, -steps), min(count, count - steps))
    return lax.ppermute(value, axis, [(source, source + steps) for source in range(leading, last)])


def banded(prev_rows, own_rows, window_len):
    blocks = own_rows.shape[0] // window_len
    joined = jnp.concatenate([prev_rows, own_rows], axis=0)
    shaped = joined.reshape((blocks + 1, window_len) + own_rows.shape[1:])
    return jnp.concatenate([shaped[:-1], shaped[1:]], axis=1)


def shards(
    residual,
    queries,
    keys,
    values,
    segments,
    routes,
    route_weight,
    sinks,
    out_weight,
    norm_gain,
    expert_gate,
    expert_up,
    expert_down,
    shared_gate,
    shared_up,
    shared_down,
):
    rows_here = residual.shape[0]
    model_width = residual.shape[1]
    tp_count = lax.axis_size("tp")
    tp_index = lax.axis_index("tp")
    head_local = queries.shape[1] // HEAD_DIM
    kv_local = keys.shape[1] // HEAD_DIM
    group_size = head_local // kv_local
    window_len = WINDOW
    blocks = rows_here // window_len
    own_marks = (segments % 256 + 1).astype(jnp.bfloat16)
    prev_keys, prev_values, prev_marks = passed_along(
        (
            keys[rows_here - window_len :],
            values[rows_here - window_len :],
            own_marks[rows_here - window_len :],
        ),
        "sp",
        1,
    )
    key_band = banded(prev_keys, keys, window_len).reshape(
        blocks, 2 * window_len, kv_local, HEAD_DIM
    )
    value_band = banded(prev_values, values, window_len).reshape(
        blocks, 2 * window_len, kv_local, HEAD_DIM
    )
    mark_band = banded(prev_marks, own_marks, window_len).astype(jnp.float32)
    query_marks = own_marks.reshape(blocks, window_len).astype(jnp.float32)
    query_blocks = queries.reshape(blocks, window_len, kv_local, group_size, HEAD_DIM)
    scores = jnp.einsum(
        "nqhgd,nkhd->nhgqk", query_blocks, key_band, preferred_element_type=jnp.float32
    ) * HEAD_DIM ** (-0.5)
    offsets = jnp.arange(window_len)[:, None] + window_len - jnp.arange(2 * window_len)[None, :]
    allowed = (
        (offsets >= 0) & (offsets < window_len) & (query_marks[:, :, None] == mark_band[:, None, :])
    )
    sink_logits = sinks.reshape(kv_local, group_size)[None, :, :, None]
    masked = jnp.where(allowed[:, None, None], scores, -jnp.inf)
    top_score = jnp.maximum(jnp.max(masked, axis=-1), sink_logits)
    exp_terms = jnp.where(allowed[:, None, None], jnp.exp(scores - top_score[..., None]), 0.0)
    denominator = jnp.sum(exp_terms, axis=-1) + jnp.exp(sink_logits - top_score)
    probabilities = (exp_terms / denominator[..., None]).astype(jnp.bfloat16)
    attended = jnp.einsum(
        "nhgqk,nkhd->nqhgd", probabilities, value_band, preferred_element_type=jnp.float32
    )
    attended = attended.astype(jnp.bfloat16).reshape(rows_here, head_local * HEAD_DIM)
    partial_value = jnp.dot(attended, out_weight, preferred_element_type=jnp.float32)
    col_width = model_width // tp_count
    col_start = tp_index * col_width
    summed = lax.psum(partial_value, "tp")
    updated = (residual.astype(jnp.float32) + summed).astype(jnp.bfloat16)
    updated_f32 = updated.astype(jnp.float32)
    inv_rms = lax.rsqrt(jnp.mean(updated_f32 * updated_f32, axis=-1, keepdims=True) + epsilon)
    normed = (updated_f32 * inv_rms * norm_gain).astype(jnp.bfloat16)
    updated_cols = lax.dynamic_slice_in_dim(updated, col_start, col_width, 1)
    normed_cols = lax.dynamic_slice_in_dim(normed, col_start, col_width, 1)
    shared_pre = jnp.dot(normed, shared_gate, preferred_element_type=jnp.float32)
    shared_lin = jnp.dot(normed, shared_up, preferred_element_type=jnp.float32)
    shared_act = (jax.nn.silu(shared_pre) * shared_lin).astype(jnp.bfloat16)
    top_count = routes.shape[1]
    experts = lax.axis_size("sp")
    capacity = 2 * rows_here * top_count // experts
    flat_ids = routes.reshape(-1)
    one_hot = (flat_ids[:, None] == jnp.arange(experts, dtype=jnp.int32)[None, :]).astype(jnp.int32)
    rank_in = jnp.cumsum(one_hot, axis=0) - one_hot
    slot_dest = flat_ids * capacity + jnp.sum(rank_in * one_hot, axis=1)
    token_of = jnp.arange(rows_here * top_count, dtype=jnp.int32) // top_count
    slot_token = jnp.full((experts * capacity,), -1, jnp.int32).at[slot_dest].set(token_of)
    filled = slot_token >= 0
    safe_token = jnp.where(filled, slot_token, 0)
    outgoing = jnp.where(filled[:, None], normed_cols[safe_token], jnp.zeros((), jnp.bfloat16))
    pieces = lax.all_to_all(
        outgoing.reshape(experts, capacity, col_width),
        "sp",
        split_axis=0,
        concat_axis=0,
        tiled=True,
    )
    arrived = lax.all_gather(pieces, "tp", axis=2, tiled=True)
    expert_rows = arrived.reshape(-1, model_width)
    gate_pre = jnp.dot(expert_rows, expert_gate[0], preferred_element_type=jnp.float32)
    up_lin = jnp.dot(expert_rows, expert_up[0], preferred_element_type=jnp.float32)
    expert_act = (jax.nn.silu(gate_pre) * up_lin).astype(jnp.bfloat16)
    gathered_expert, gathered_shared = (
        lax.all_gather(expert_act, "tp", axis=1, tiled=True),
        lax.all_gather(shared_act, "tp", axis=1, tiled=True),
    )
    expert_out = jnp.dot(
        gathered_expert, expert_down[0], preferred_element_type=jnp.float32
    ).astype(jnp.bfloat16)
    returned = lax.all_to_all(
        expert_out.reshape(experts, capacity, col_width),
        "sp",
        split_axis=0,
        concat_axis=0,
        tiled=True,
    )
    returned = returned.reshape(experts * capacity, col_width)
    picked = returned[slot_dest].astype(jnp.float32).reshape(rows_here, top_count, col_width)
    routed = jnp.sum(picked * route_weight[:, :, None], axis=1)
    shared_cols = jnp.dot(gathered_shared, shared_down, preferred_element_type=jnp.float32)
    return (updated_cols.astype(jnp.float32) + shared_cols + routed).astype(jnp.bfloat16)


def solution(mesh):
    placed = (
        P(("grp", "sp"), None),
        P(("grp", "sp"), "tp"),
        P(("grp", "sp"), "tp"),
        P(("grp", "sp"), "tp"),
        P(("grp", "sp")),
        P(("grp", "sp"), None),
        P(("grp", "sp"), None),
        P("tp"),
        P("tp", None),
        P(),
        P("sp", None, "tp"),
        P("sp", None, "tp"),
        P("sp", None, "tp"),
        P(None, "tp"),
        P(None, "tp"),
        P(None, "tp"),
    )
    return jax.shard_map(
        shards, mesh=mesh, in_specs=placed, out_specs=P(("grp", "sp"), "tp"), check_vma=False
    )
```

profile of v0, /device:TPU:0, one launch (start us, length us, event | category | flops | bytes accessed | tf_op | source)
XLA Modules:
  0.0 231.0 jit_solution(2736606239957524361)
XLA Ops:
  7.3 5.0 %collective-permute-start.1 = (bf16[128]{0:T(256)(128)(2,1)S(1)}, bf16[128]{0:T(256)(128)(2,1)S(1)}, u32[]{:S(2)}, u32[]{:S(2)}) collective-permute-start(bf16[128]{0:T(256)(128)(2,1)S(1)} %slice.47), channel_id=1, source_target_pairs={{0,4},{4,8},{8,12},{1,5},{5,9},{9,13},{2,6},{6,10},{10,14},{3,7},{... | collective-permute-start | bytes 776 | tf_op jit(solution)/shard_map/ppermute | solution.py:14
  13.1 3.5 %collective-permute-start.2 = (bf16[128,128]{1,0:T(8,128)(2,1)S(1)}, bf16[128,128]{1,0:T(8,128)(2,1)S(1)}, u32[]{:S(2)}, u32[]{:S(2)}) collective-permute-start(bf16[128,128]{1,0:T(8,128)(2,1)S(1)} %slice.50), channel_id=1, source_target_pairs={{0,4},{4,8},{8,12},{1,5},{5,9},{9,13},{2,6},{6,10},{10,14},{3,7},{... | collective-permute-start | bytes 98312 | tf_op jit(solution)/shard_map/ppermute | solution.py:14
  17.3 3.5 %collective-permute-start = (bf16[128,128]{1,0:T(8,128)(2,1)S(1)}, bf16[128,128]{1,0:T(8,128)(2,1)S(1)}, u32[]{:S(2)}, u32[]{:S(2)}) collective-permute-start(bf16[128,128]{1,0:T(8,128)(2,1)S(1)} %slice.45), channel_id=1, source_target_pairs={{0,4},{4,8},{8,12},{1,5},{5,9},{9,13},{2,6},{6,10},{10,14},{3,7},{... | collective-permute-start | bytes 98312 | tf_op jit(solution)/shard_map/ppermute | solution.py:14
  24.4 1.2 reduce-window.6
  25.8 1.1 reshape.216
  30.6 1.8 fusion.15
  33.2 2.4 %scatter_custom_fusion = s32[1024]{0:T(1024)S(1)} fusion(s32[512]{0:T(512)S(1)} %bitcast.75, s32[512]{0:T(512)S(1)} %add_select_fusion, s32[]{:T(128)} %constant.70.clone.1), kind=kCustom, calls=%fused_computation.71 | custom fusion | bytes 4100 | tf_op jit(solution)/shard_map/scatter | solution.py:108
  35.7 46.5 %all-reduce.2.cloned.1.call-done = f32[256,2048]{1,0:T(8,128)} async-done(((f32[256,2048]{1,0:T(8,128)}), f32[256,2048]{1,0:T(8,128)}) %all-reduce.2.cloned.1.call-update) | async-done | bytes 2097168 | tf_op jit(solution)/shard_map/psum | solution.py:90
  82.2 2.0 fusion
  85.5 4.0 %gather_fusion = bf16[1024,512]{1,0:T(8,128)(2,1)S(1)} fusion(bf16[256,512]{1,0:T(8,128)(2,1)S(1)} %constant_dynamic-slice_fusion, s32[1024]{0:T(1024)S(1)} %fusion.29), kind=kCustom, calls=%fused_computation | custom fusion | bytes 2101248 | tf_op jit(solution)/shard_map/gather | solution.py:111
  89.7 30.1 %all_to_all.10 = bf16[4,256,512]{2,1,0:T(8,128)(2,1)} all-to-all(bf16[4,256,512]{2,1,0:T(8,128)(2,1)S(1)} %broadcast_select_fusion), channel_id=1, replica_groups=mesh['grp'=2,'sp'=4,'tp'=4] {'sp'}, dimensions={0} | all-to-all | bytes 2097152 | tf_op jit(solution)/shard_map/all_to_all | solution.py:112
  119.9 32.9 %all-gather.3.cloned.1.call-done = bf16[4,256,2048]{2,1,0:T(8,128)(2,1)} async-done(((bf16[4,256,512]{2,1,0:T(8,128)(2,1)}), bf16[4,256,2048]{2,1,0:T(8,128)(2,1)}) %all-gather.3.cloned.1.call-update) | async-done | bytes 4194320 | tf_op jit(solution)/shard_map/all_gather | solution.py:119
  152.8 3.6 %fusion.11 = f32[1024,256]{1,0:T(8,128)S(1)} fusion(bf16[1024,2048]{1,0:T(8,128)(2,1)} %bitcast.80, bf16[1,2048,256]{2,1,0:T(8,128)(2,1)S(1)} %copy-done.8), kind=kOutput, calls=%fused_computation.23 | convolution fusion | flops 1073741824 | bytes 6291456 | tf_op jit(solution)/shard_map/dot_general | solution.py:121
  156.5 2.1 fusion.4
  158.6 23.0 %all-gather.5.cloned.1.call-done = bf16[1024,1024]{1,0:T(8,128)(2,1)} async-done(((bf16[1024,256]{1,0:T(8,128)(2,1)}), bf16[1024,1024]{1,0:T(8,128)(2,1)}) %all-gather.5.cloned.1.call-update) | async-done | bytes 2097168 | tf_op jit(solution)/shard_map/all_gather | solution.py:125
  181.6 3.9 %convolution_convert_fusion = bf16[1024,512]{1,0:T(8,128)(2,1)} fusion(bf16[1024,1024]{1,0:T(8,128)(2,1)} %all-gather.5.cloned.1.call-done, bf16[1,1024,512]{2,1,0:T(8,128)(2,1)S(1)} %copy-done.10), kind=kOutput, calls=%fused_computation.9 | convolution fusion | flops 1074266112 | bytes 4194304 | tf_op jit(solution)/shard_map/dot_general | solution.py:128
  185.5 4.7 %all-to-all-start.1 = ((bf16[4,256,512]{2,1,0:T(8,128)(2,1)}), bf16[4,256,512]{2,1,0:T(8,128)(2,1)S(1)}, u32[]{:S(2)}, u32[]{:S(2)}) async-start(bf16[4,256,512]{2,1,0:T(8,128)(2,1)} %bitcast.73), calls=%async_computation.1 | async-start | bytes 2097152 | tf_op jit(solution)/shard_map/all_to_all | solution.py:131
  190.3 2.1 fusion.42
  192.9 7.5 %all_gather.9 = bf16[256,1024]{1,0:T(8,128)(2,1)} all-gather(bf16[256,256]{1,0:T(8,128)(2,1)S(1)} %fusion.7), channel_id=1, replica_groups=mesh['grp'=2,'sp'=4,'tp'=4] {'tp'}, dimensions={1}, use_global_device_ids=true | all-gather | bytes 655360 | tf_op jit(solution)/shard_map/all_gather | solution.py:126
  200.5 15.8 %all-to-all-done.1 = bf16[4,256,512]{2,1,0:T(8,128)(2,1)S(1)} async-done(((bf16[4,256,512]{2,1,0:T(8,128)(2,1)}), bf16[4,256,512]{2,1,0:T(8,128)(2,1)S(1)}, u32[]{:S(2)}, u32[]{:S(2)}) %all-to-all-start.1) | async-done | bytes 1048608 | tf_op jit(solution)/shard_map/all_to_all | solution.py:131
  216.3 2.6 %gather_fusion.1 = bf16[512,512]{1,0:T(8,128)(2,1)} fusion(bf16[1024,512]{1,0:T(8,128)(2,1)S(1)} %bitcast.71, s32[1024]{0:T(1024)S(1)} %pad_clamp_fusion), kind=kCustom, calls=%fused_computation.1 | custom fusion | bytes 1050624 | tf_op jit(solution)/shard_map/gather | solution.py:139
  218.9 1.7 reshape.184
  220.6 1.3 multiply_reduce_fusion
  222.0 2.5 %fusion.6 = bf16[256,512]{1,0:T(8,128)(2,1)} fusion(f32[256,512]{1,0:T(8,128)S(1)} %multiply_reduce_fusion, bf16[256,1024]{1,0:T(8,128)(2,1)} %all_gather.9, bf16[1024,512]{1,0:T(8,128)(2,1)} %param.31, bf16[256,2048]{1,0:T(8,128)(2,1)S(1)} %get-tuple-element.6, s32[]{:T(128)S(6)} %select_n.49), kind=kOutput, calls=%fused_computation.16 | convolution fusion | flops 268959744 | bytes 2621444 | tf_op jit(solution)/shard_map/dot_general | solution.py:141
  (83 shorter events, 12.7 us)
Async XLA Ops:
  6.5 24.1 %copy-start = (bf16[256,2048]{1,0:T(8,128)(2,1)S(1)}, bf16[256,2048]{1,0:T(8,128)(2,1)}, u32[]{:S(2)}) copy-start(bf16[256,2048]{1,0:T(8,128)(2,1)} %param.24) | copy-start | bytes 3145732
  6.5 75.6 %all-reduce.2.cloned.1.call-start = ((), (), s32[]{:S(2)}) async-start(), calls=%async_computation.2 | async-start | bytes 4194304 | tf_op jit(solution)/shard_map/psum | solution.py:90
  7.3 20.6 %collective-permute-start.1 = (bf16[128]{0:T(256)(128)(2,1)S(1)}, bf16[128]{0:T(256)(128)(2,1)S(1)}, u32[]{:S(2)}, u32[]{:S(2)}) collective-permute-start(bf16[128]{0:T(256)(128)(2,1)S(1)} %slice.47), channel_id=1, source_target_pairs={{0,4},{4,8},{8,12},{1,5},{5,9},{9,13},{2,6},{6,10},{10,14},{3,7},{... | collective-permute-start | bytes 776 | tf_op jit(solution)/shard_map/ppermute | solution.py:14
  13.1 15.0 %collective-permute-start.2 = (bf16[128,128]{1,0:T(8,128)(2,1)S(1)}, bf16[128,128]{1,0:T(8,128)(2,1)S(1)}, u32[]{:S(2)}, u32[]{:S(2)}) collective-permute-start(bf16[128,128]{1,0:T(8,128)(2,1)S(1)} %slice.50), channel_id=1, source_target_pairs={{0,4},{4,8},{8,12},{1,5},{5,9},{9,13},{2,6},{6,10},{10,14},{3,7},{... | collective-permute-start | bytes 98312 | tf_op jit(solution)/shard_map/ppermute | solution.py:14
  17.3 12.5 %collective-permute-start = (bf16[128,128]{1,0:T(8,128)(2,1)S(1)}, bf16[128,128]{1,0:T(8,128)(2,1)S(1)}, u32[]{:S(2)}, u32[]{:S(2)}) collective-permute-start(bf16[128,128]{1,0:T(8,128)(2,1)S(1)} %slice.45), channel_id=1, source_target_pairs={{0,4},{4,8},{8,12},{1,5},{5,9},{9,13},{2,6},{6,10},{10,14},{3,7},{... | collective-permute-start | bytes 98312 | tf_op jit(solution)/shard_map/ppermute | solution.py:14
  25.8 4.0 %copy-start.4 = (bf16[256,128]{1,0:T(8,128)(2,1)S(1)}, bf16[256,128]{1,0:T(8,128)(2,1)}, u32[]{:S(2)}) copy-start(bf16[256,128]{1,0:T(8,128)(2,1)} %param.19) | copy-start | bytes 196612
  32.4 49.8 %copy-start.3 = (bf16[256,2048]{1,0:T(8,128)(2,1)S(1)}, bf16[256,2048]{1,0:T(8,128)(2,1)}, u32[]{:S(2)}) copy-start(bf16[256,2048]{1,0:T(8,128)(2,1)} %param.16) | copy-start | bytes 3145732
  32.4 120.4 %all-gather.3.cloned.1.call-start = ((), (), s32[]{:S(2)}) async-start(), calls=%async_computation.3 | async-start | bytes 5242880 | tf_op jit(solution)/shard_map/all_gather | solution.py:119
  35.7 48.5 %copy-start.5 = (f32[2048]{0:T(1024)S(1)}, f32[2048]{0:T(1024)}, u32[]{:S(2)}) copy-start(f32[2048]{0:T(1024)} %param.25) | copy-start | bytes 24580
  84.5 1.0 copy-start.1
  89.6 63.1 %copy-start.8 = (bf16[1,2048,256]{2,1,0:T(8,128)(2,1)S(1)}, bf16[1,2048,256]{2,1,0:T(8,128)(2,1)}, u32[]{:S(2)}) copy-start(bf16[1,2048,256]{2,1,0:T(8,128)(2,1)} %param.26) | copy-start | bytes 3145732
  119.8 61.8 %all-gather.5.cloned.1.call-start = ((), (), s32[]{:S(2)}) async-start(), calls=%async_computation.4 | async-start | bytes 2621440 | tf_op jit(solution)/shard_map/all_gather | solution.py:125
  152.8 3.6 %copy-start.7 = (bf16[4,256,2048]{2,1,0:T(8,128)(2,1)S(1)}, bf16[4,256,2048]{2,1,0:T(8,128)(2,1)}, u32[]{:S(2)}) copy-start(bf16[4,256,2048]{2,1,0:T(8,128)(2,1)} %all-gather.3.cloned.1.call-done) | copy-start | bytes 12582916
  152.8 3.7 %copy-start.9 = (bf16[1,2048,256]{2,1,0:T(8,128)(2,1)S(1)}, bf16[1,2048,256]{2,1,0:T(8,128)(2,1)}, u32[]{:S(2)}) copy-start(bf16[1,2048,256]{2,1,0:T(8,128)(2,1)} %param.27) | copy-start | bytes 3145732
  156.5 25.1 %copy-start.10 = (bf16[1,1024,512]{2,1,0:T(8,128)(2,1)S(1)}, bf16[1,1024,512]{2,1,0:T(8,128)(2,1)}, u32[]{:S(2)}) copy-start(bf16[1,1024,512]{2,1,0:T(8,128)(2,1)} %param.28) | copy-start | bytes 3145732
  185.5 4.7 %copy-start.6 = (f32[256,2]{0,1:T(2,128)S(1)}, f32[256,2]{0,1:T(2,128)}, u32[]{:S(2)}) copy-start(f32[256,2]{0,1:T(2,128)} %param.22) | copy-start | bytes 6148
  185.5 30.8 %all-to-all-start.1 = ((bf16[4,256,512]{2,1,0:T(8,128)(2,1)}), bf16[4,256,512]{2,1,0:T(8,128)(2,1)S(1)}, u32[]{:S(2)}, u32[]{:S(2)}) async-start(bf16[4,256,512]{2,1,0:T(8,128)(2,1)} %bitcast.73), calls=%async_computation.1 | async-start | bytes 2097152 | tf_op jit(solution)/shard_map/all_to_all | solution.py:131
  190.3 2.2 copy-start.2
  190.3 2.2 copy-start.11
Sparse Core Ops, SparseCore 0:
  32.5 49.5 all-reduce.1
  119.9 32.7 all-gather.2
  158.8 22.8 all-gather.4
where the time goes:
time: 232 us; the launch traced here: 231 us
  waiting for transfers between devices  118 us (51%)
  blocking collectives  37.7 us (16%)
  local copies, waits for them, and re-layouts  19.6 us (8%)
  matrix products  17.1 us (7%)
  starting transfers between devices  16.7 us (7%)
  between operations  13.5 us (6%)
  other arithmetic  8.15 us (4%)
    psum x1, waiting for transfers between devices, shards(): summed = lax.psum(partial_value, 'tp')  46.5 us
    all_gather x1, waiting for transfers between devices, shards(): arrived = lax.all_gather(pieces, 'tp', axis=2, tiled=True)  32.9 us
    all_to_all x1, blocking collectives, shards(): lax.all_to_all(outgoing.reshape(experts, capacity, col_width), 'sp', spli...  30.1 us
    all_gather x1, waiting for transfers between devices, shards(): lax.all_gather(expert_act, 'tp', axis=1, tiled=True)  23 us
    all_to_all x1, waiting for transfers between devices, shards(): lax.all_to_all(expert_out.reshape(experts, capacity, col_width), 'sp', sp...  15.8 us
    ppermute x3, starting transfers between devices, passed_along(): lax.ppermute(value, axis, [(source, source + steps) for source in range(l...  11.9 us
    all_gather x1, blocking collectives, shards(): lax.all_gather(shared_act, 'tp', axis=1, tiled=True)  7.53 us
    all_to_all x1, starting transfers between devices, shards(): lax.all_to_all(expert_out.reshape(experts, capacity, col_width), 'sp', sp...  4.71 us
  transfers between devices with their start and end apart: 7, of which 4 were waited for; matrix products, arithmetic and copies ran while one was open for 7% of the time, Pallas kernels for 0%

commit v1 on v0

--- a/solution.py
+++ b/solution.py
@@ -87,7 +87,8 @@
     partial_value = jnp.dot(attended, out_weight, preferred_element_type=jnp.float32)
     col_width = model_width // tp_count
     col_start = tp_index * col_width
-    summed = lax.psum(partial_value, "tp")
+    store_records_in = lambda body: jnp.sum(jax.lax.all_gather(body, "tp"), 0)
+    summed = store_records_in(partial_value)
     updated = (residual.astype(jnp.float32) + summed).astype(jnp.bfloat16)
     updated_f32 = updated.astype(jnp.float32)
     inv_rms = lax.rsqrt(jnp.mean(updated_f32 * updated_f32, axis=-1, keepdims=True) + epsilon)

time: 232 us -> 240 us (1.034)
  waiting for transfers between devices: 118 us -> 124 us
  other arithmetic: 8.15 us -> 11.5 us
    all_gather x0 -> x1, waiting for transfers between devices: none -> 51.6 us  [shards(): store_records_in = lambda body: jnp.sum(jax.lax.all_gather(body, 'tp'), 0)]
    psum x1 -> x0, waiting for transfers between devices: 46.5 us -> none  [shards(): summed = lax.psum(partial_value, 'tp')]
    reduce_sum x0 -> x1, other arithmetic: none -> 4.4 us  [shards(): store_records_in = lambda body: jnp.sum(jax.lax.all_gather(body, 'tp'), 0)]
  transfers between devices with their start and end apart: 7 -> 7, of which waited for: 4 -> 4; matrix products, arithmetic and copies ran while one was open for 7% -> 6% of each run, Pallas kernels for 0% -> 0%
where the time goes in v1:
time: 240 us; the launch traced here: 239 us
  waiting for transfers between devices  124 us (52%)
  blocking collectives  38.3 us (16%)
  local copies, waits for them, and re-layouts  19 us (8%)
  starting transfers between devices  16.7 us (7%)
  matrix products  16.7 us (7%)
  between operations  13.6 us (6%)
  other arithmetic  11.5 us (5%)
    all_gather x1, waiting for transfers between devices, shards(): store_records_in = lambda body: jnp.sum(jax.lax.all_gather(body, 'tp'), 0)  51.6 us
    all_gather x1, waiting for transfers between devices, shards(): arrived = lax.all_gather(pieces, 'tp', axis=2, tiled=True)  32.7 us
    all_to_all x1, blocking collectives, shards(): lax.all_to_all(outgoing.reshape(experts, capacity, col_width), 'sp', spli...  30.8 us
    all_gather x1, waiting for transfers between devices, shards(): lax.all_gather(expert_act, 'tp', axis=1, tiled=True)  23 us
    all_to_all x1, waiting for transfers between devices, shards(): lax.all_to_all(expert_out.reshape(experts, capacity, col_width), 'sp', sp...  16.2 us
    ppermute x3, starting transfers between devices, passed_along(): lax.ppermute(value, axis, [(source, source + steps) for source in range(l...  11.9 us
    all_gather x1, blocking collectives, shards(): lax.all_gather(shared_act, 'tp', axis=1, tiled=True)  7.54 us
  transfers between devices with their start and end apart: 7, of which 4 were waited for; matrix products, arithmetic and copies ran while one was open for 6% of the time, Pallas kernels for 0%

profile of v1, /device:TPU:0, one launch (start us, length us, event | category | flops | bytes accessed | tf_op | source)
XLA Modules:
  0.0 239.3 jit_solution(10419939031764097993)
XLA Ops:
  7.3 5.0 %collective-permute-start.1 = (bf16[128]{0:T(256)(128)(2,1)S(1)}, bf16[128]{0:T(256)(128)(2,1)S(1)}, u32[]{:S(2)}, u32[]{:S(2)}) collective-permute-start(bf16[128]{0:T(256)(128)(2,1)S(1)} %slice.47), channel_id=1, source_target_pairs={{0,4},{4,8},{8,12},{1,5},{5,9},{9,13},{2,6},{6,10},{10,14},{3,7},{... | collective-permute-start | bytes 776 | tf_op jit(solution)/shard_map/ppermute | solution.py:14
  13.1 3.5 %collective-permute-start.2 = (bf16[128,128]{1,0:T(8,128)(2,1)S(1)}, bf16[128,128]{1,0:T(8,128)(2,1)S(1)}, u32[]{:S(2)}, u32[]{:S(2)}) collective-permute-start(bf16[128,128]{1,0:T(8,128)(2,1)S(1)} %slice.50), channel_id=1, source_target_pairs={{0,4},{4,8},{8,12},{1,5},{5,9},{9,13},{2,6},{6,10},{10,14},{3,7},{... | collective-permute-start | bytes 98312 | tf_op jit(solution)/shard_map/ppermute | solution.py:14
  17.3 3.5 %collective-permute-start = (bf16[128,128]{1,0:T(8,128)(2,1)S(1)}, bf16[128,128]{1,0:T(8,128)(2,1)S(1)}, u32[]{:S(2)}, u32[]{:S(2)}) collective-permute-start(bf16[128,128]{1,0:T(8,128)(2,1)S(1)} %slice.45), channel_id=1, source_target_pairs={{0,4},{4,8},{8,12},{1,5},{5,9},{9,13},{2,6},{6,10},{10,14},{3,7},{... | collective-permute-start | bytes 98312 | tf_op jit(solution)/shard_map/ppermute | solution.py:14
  27.5 1.9 fusion.15
  29.9 1.2 reduce-window.6
  31.9 2.4 %scatter_custom_fusion = s32[1024]{0:T(1024)S(1)} fusion(s32[512]{0:T(512)S(1)} %bitcast.77, s32[512]{0:T(512)S(1)} %add_select_fusion, s32[]{:T(128)} %constant.70.clone.1), kind=kCustom, calls=%fused_computation.71 | custom fusion | bytes 4100 | tf_op jit(solution)/shard_map/scatter | solution.py:109
  34.4 51.6 %all-gather.9.cloned.1.call-done = f32[1024,2048]{1,0:T(8,128)} async-done(((f32[256,2048]{1,0:T(8,128)}), f32[1024,2048]{1,0:T(8,128)}) %all-gather.9.cloned.1.call-update) | async-done | bytes 8388624 | tf_op jit(solution)/shard_map/all_gather | solution.py:90
  86.0 4.4 %reduce_sum.48 = f32[256,2048]{1,0:T(8,128)S(1)} reduce(f32[4,256,2048]{2,1,0:T(8,128)} %bitcast.73, f32[]{:T(128)} %constant.63.clone.1), dimensions={0}, to_apply=%region_2.3 | reduce | flops 1572864 | bytes 10485764 | tf_op jit(solution)/shard_map/reduce_sum | solution.py:90
  90.4 1.6 fusion
  93.4 4.0 %gather_fusion = bf16[1024,512]{1,0:T(8,128)(2,1)S(1)} fusion(bf16[256,512]{1,0:T(8,128)(2,1)S(1)} %constant_dynamic-slice_fusion, s32[1024]{0:T(1024)S(1)} %fusion.29), kind=kCustom, calls=%fused_computation | custom fusion | bytes 2101248 | tf_op jit(solution)/shard_map/gather | solution.py:112
  97.6 30.8 %all_to_all.10 = bf16[4,256,512]{2,1,0:T(8,128)(2,1)} all-to-all(bf16[4,256,512]{2,1,0:T(8,128)(2,1)S(1)} %broadcast_select_fusion), channel_id=1, replica_groups=mesh['grp'=2,'sp'=4,'tp'=4] {'sp'}, dimensions={0} | all-to-all | bytes 2097152 | tf_op jit(solution)/shard_map/all_to_all | solution.py:113
  128.4 32.7 %all-gather.5.cloned.1.call-done = bf16[4,256,2048]{2,1,0:T(8,128)(2,1)} async-done(((bf16[4,256,512]{2,1,0:T(8,128)(2,1)}), bf16[4,256,2048]{2,1,0:T(8,128)(2,1)}) %all-gather.5.cloned.1.call-update) | async-done | bytes 4194320 | tf_op jit(solution)/shard_map/all_gather | solution.py:120
  161.1 3.6 %fusion.11 = f32[1024,256]{1,0:T(8,128)S(1)} fusion(bf16[1024,2048]{1,0:T(8,128)(2,1)} %bitcast.82, bf16[1,2048,256]{2,1,0:T(8,128)(2,1)S(1)} %copy-done.8), kind=kOutput, calls=%fused_computation.23 | convolution fusion | flops 1073741824 | bytes 6291456 | tf_op jit(solution)/shard_map/dot_general | solution.py:122
  164.9 2.1 fusion.4
  167.0 23.0 %all-gather.7.cloned.1.call-done = bf16[1024,1024]{1,0:T(8,128)(2,1)} async-done(((bf16[1024,256]{1,0:T(8,128)(2,1)}), bf16[1024,1024]{1,0:T(8,128)(2,1)}) %all-gather.7.cloned.1.call-update) | async-done | bytes 2097168 | tf_op jit(solution)/shard_map/all_gather | solution.py:126
  189.9 3.8 %convolution_convert_fusion = bf16[1024,512]{1,0:T(8,128)(2,1)} fusion(bf16[1024,1024]{1,0:T(8,128)(2,1)} %all-gather.7.cloned.1.call-done, bf16[1,1024,512]{2,1,0:T(8,128)(2,1)S(1)} %copy-done.10), kind=kOutput, calls=%fused_computation.9 | convolution fusion | flops 1074266112 | bytes 4194304 | tf_op jit(solution)/shard_map/dot_general | solution.py:129
  193.8 4.7 %all-to-all-start.1 = ((bf16[4,256,512]{2,1,0:T(8,128)(2,1)}), bf16[4,256,512]{2,1,0:T(8,128)(2,1)S(1)}, u32[]{:S(2)}, u32[]{:S(2)}) async-start(bf16[4,256,512]{2,1,0:T(8,128)(2,1)} %bitcast.75), calls=%async_computation.1 | async-start | bytes 2097152 | tf_op jit(solution)/shard_map/all_to_all | solution.py:132
  198.7 1.7 fusion.42
  200.9 7.5 %all_gather.17 = bf16[256,1024]{1,0:T(8,128)(2,1)} all-gather(bf16[256,256]{1,0:T(8,128)(2,1)S(1)} %fusion.7), channel_id=1, replica_groups=mesh['grp'=2,'sp'=4,'tp'=4] {'tp'}, dimensions={1}, use_global_device_ids=true | all-gather | bytes 655360 | tf_op jit(solution)/shard_map/all_gather | solution.py:127
  208.4 16.2 %all-to-all-done.1 = bf16[4,256,512]{2,1,0:T(8,128)(2,1)S(1)} async-done(((bf16[4,256,512]{2,1,0:T(8,128)(2,1)}), bf16[4,256,512]{2,1,0:T(8,128)(2,1)S(1)}, u32[]{:S(2)}, u32[]{:S(2)}) %all-to-all-start.1) | async-done | bytes 1048608 | tf_op jit(solution)/shard_map/all_to_all | solution.py:132
  224.7 2.6 %gather_fusion.1 = bf16[512,512]{1,0:T(8,128)(2,1)} fusion(bf16[1024,512]{1,0:T(8,128)(2,1)S(1)} %bitcast.72, s32[1024]{0:T(1024)S(1)} %pad_clamp_fusion), kind=kCustom, calls=%fused_computation.1 | custom fusion | bytes 1050624 | tf_op jit(solution)/shard_map/gather | solution.py:140
  227.3 1.8 reshape.184
  229.0 1.3 multiply_reduce_fusion
  230.4 2.4 %fusion.6 = bf16[256,512]{1,0:T(8,128)(2,1)} fusion(f32[256,512]{1,0:T(8,128)S(1)} %multiply_reduce_fusion, bf16[256,1024]{1,0:T(8,128)(2,1)S(1)} %copy-done.2, bf16[1024,512]{1,0:T(8,128)(2,1)} %param.31, bf16[256,2048]{1,0:T(8,128)(2,1)} %copy-done.1, s32[]{:T(128)S(6)} %select_n.49), kind=kOutput, calls=%fused_computation.16 | convolution fusion | flops 268959744 | bytes 2621444 | tf_op jit(solution)/shard_map/dot_general | solution.py:142
  (84 shorter events, 12.5 us)
Async XLA Ops:
  6.5 21.0 %copy-start = (bf16[256,2048]{1,0:T(8,128)(2,1)S(1)}, bf16[256,2048]{1,0:T(8,128)(2,1)}, u32[]{:S(2)}) copy-start(bf16[256,2048]{1,0:T(8,128)(2,1)} %param.24) | copy-start | bytes 3145732
  6.5 79.5 %all-gather.9.cloned.1.call-start = ((), (), s32[]{:S(2)}) async-start(), calls=%async_computation.4 | async-start | bytes 10485760 | tf_op jit(solution)/shard_map/all_gather | solution.py:90
  7.3 17.5 %collective-permute-start.1 = (bf16[128]{0:T(256)(128)(2,1)S(1)}, bf16[128]{0:T(256)(128)(2,1)S(1)}, u32[]{:S(2)}, u32[]{:S(2)}) collective-permute-start(bf16[128]{0:T(256)(128)(2,1)S(1)} %slice.47), channel_id=1, source_target_pairs={{0,4},{4,8},{8,12},{1,5},{5,9},{9,13},{2,6},{6,10},{10,14},{3,7},{... | collective-permute-start | bytes 776 | tf_op jit(solution)/shard_map/ppermute | solution.py:14
  13.1 12.0 %collective-permute-start.2 = (bf16[128,128]{1,0:T(8,128)(2,1)S(1)}, bf16[128,128]{1,0:T(8,128)(2,1)S(1)}, u32[]{:S(2)}, u32[]{:S(2)}) collective-permute-start(bf16[128,128]{1,0:T(8,128)(2,1)S(1)} %slice.50), channel_id=1, source_target_pairs={{0,4},{4,8},{8,12},{1,5},{5,9},{9,13},{2,6},{6,10},{10,14},{3,7},{... | collective-permute-start | bytes 98312 | tf_op jit(solution)/shard_map/ppermute | solution.py:14
  17.3 9.4 %collective-permute-start = (bf16[128,128]{1,0:T(8,128)(2,1)S(1)}, bf16[128,128]{1,0:T(8,128)(2,1)S(1)}, u32[]{:S(2)}, u32[]{:S(2)}) collective-permute-start(bf16[128,128]{1,0:T(8,128)(2,1)S(1)} %slice.45), channel_id=1, source_target_pairs={{0,4},{4,8},{8,12},{1,5},{5,9},{9,13},{2,6},{6,10},{10,14},{3,7},{... | collective-permute-start | bytes 98312 | tf_op jit(solution)/shard_map/ppermute | solution.py:14
  22.7 4.0 %copy-start.3 = (bf16[256,128]{1,0:T(8,128)(2,1)S(1)}, bf16[256,128]{1,0:T(8,128)(2,1)}, u32[]{:S(2)}) copy-start(bf16[256,128]{1,0:T(8,128)(2,1)} %param.19) | copy-start | bytes 196612
  27.5 1.9 copy-start.5
  29.4 131.7 %all-gather.5.cloned.1.call-start = ((), (), s32[]{:S(2)}) async-start(), calls=%async_computation.2 | async-start | bytes 5242880 | tf_op jit(solution)/shard_map/all_gather | solution.py:120
  90.4 2.6 %copy-start.4 = (f32[2048]{0:T(1024)S(1)}, f32[2048]{0:T(1024)}, u32[]{:S(2)}) copy-start(f32[2048]{0:T(1024)} %param.25) | copy-start | bytes 24580
  92.1 1.0 copy-start.1
  97.6 63.6 %copy-start.8 = (bf16[1,2048,256]{2,1,0:T(8,128)(2,1)S(1)}, bf16[1,2048,256]{2,1,0:T(8,128)(2,1)}, u32[]{:S(2)}) copy-start(bf16[1,2048,256]{2,1,0:T(8,128)(2,1)} %param.26) | copy-start | bytes 3145732
  128.4 61.6 %all-gather.7.cloned.1.call-start = ((), (), s32[]{:S(2)}) async-start(), calls=%async_computation.3 | async-start | bytes 2621440 | tf_op jit(solution)/shard_map/all_gather | solution.py:126
  161.1 3.6 %copy-start.7 = (bf16[4,256,2048]{2,1,0:T(8,128)(2,1)S(1)}, bf16[4,256,2048]{2,1,0:T(8,128)(2,1)}, u32[]{:S(2)}) copy-start(bf16[4,256,2048]{2,1,0:T(8,128)(2,1)} %all-gather.5.cloned.1.call-done) | copy-start | bytes 12582916
  161.1 3.7 %copy-start.9 = (bf16[1,2048,256]{2,1,0:T(8,128)(2,1)S(1)}, bf16[1,2048,256]{2,1,0:T(8,128)(2,1)}, u32[]{:S(2)}) copy-start(bf16[1,2048,256]{2,1,0:T(8,128)(2,1)} %param.27) | copy-start | bytes 3145732
  164.9 25.1 %copy-start.10 = (bf16[1,1024,512]{2,1,0:T(8,128)(2,1)S(1)}, bf16[1,1024,512]{2,1,0:T(8,128)(2,1)}, u32[]{:S(2)}) copy-start(bf16[1,1024,512]{2,1,0:T(8,128)(2,1)} %param.28) | copy-start | bytes 3145732
  193.8 4.7 %copy-start.6 = (f32[256,2]{0,1:T(2,128)S(1)}, f32[256,2]{0,1:T(2,128)}, u32[]{:S(2)}) copy-start(f32[256,2]{0,1:T(2,128)} %param.22) | copy-start | bytes 6148
  193.8 30.9 %all-to-all-start.1 = ((bf16[4,256,512]{2,1,0:T(8,128)(2,1)}), bf16[4,256,512]{2,1,0:T(8,128)(2,1)S(1)}, u32[]{:S(2)}, u32[]{:S(2)}) async-start(bf16[4,256,512]{2,1,0:T(8,128)(2,1)} %bitcast.75), calls=%async_computation.1 | async-start | bytes 2097152 | tf_op jit(solution)/shard_map/all_to_all | solution.py:132
  198.6 1.8 copy-start.11
  227.3 3.1 %copy-start.2 = (bf16[256,1024]{1,0:T(8,128)(2,1)S(1)}, bf16[256,1024]{1,0:T(8,128)(2,1)}, u32[]{:S(2)}) copy-start(bf16[256,1024]{1,0:T(8,128)(2,1)} %all_gather.17) | copy-start | bytes 1572868
Sparse Core Ops, SparseCore 0:
  29.5 56.4 all-gather.8
  128.5 32.5 all-gather.4
  167.1 22.8 all-gather.6
